TPU v7x, 32 devices: a whole 2x2x4 slice. The times are simulated.
32 devices in a mesh: sp: 8 (over z, y), tp: 4 (over x, core).
Axes of the slice: x: 2, y: 2, z: 4, core: 2. Of those that a mesh axis runs over, the one named last changes fastest.
Arguments:
- latent: bfloat16 [3072, 2048], P(('sp', 'tp')), may hold values from -6 to 6
- context: bfloat16 [512, 2048], P('sp'), may hold values from -6 to 6
- cond_latent: float32 [2048], replicated, may hold values from -6 to 6
- cond_context: float32 [2048], replicated, may hold values from -12 to 12
- shift_weight: bfloat16 [2048, 2048], P('sp', 'tp'), may hold values from -0.125 to 0.125
- scale_weight: bfloat16 [2048, 2048], P('sp', 'tp'), may hold values from -0.125 to 0.125
- gate_weight: bfloat16 [2048, 2048], P('sp', 'tp'), may hold values from -0.125 to 0.125
- query_weight: bfloat16 [2, 2048, 1024], P(None, None, 'tp'), may hold values from -1.3258252 to 1.3258252
- key_weight: bfloat16 [2, 2048, 1024], P(None, None, 'tp'), may hold values from -1.3258252 to 1.3258252
- value_weight: bfloat16 [2048, 2048], P(None, 'tp'), may hold values from -0.125 to 0.125
- out_weight: bfloat16 [2048, 2048], P('tp'), may hold values from -0.125 to 0.125
- lambda_heads: float32 [16], P('tp'), may hold values from 0.3 to 0.8
- out_gain: float32 [2048], P('tp'), may hold values from 0.1 to 1.9
Outputs:
- result: bfloat16 [3072, 2048], P(('sp', 'tp'))
All inputs are finite; a program needn't handle non-finite values.
Results may differ from a plain program's by a relative error of at most 0.02.
The roundings to bfloat16 on the way count: a program that leaves them out, or rounds other values in their place, can miss the bound.
Values may be sent and summed in bfloat16 or wider, within the bound.
A program may use at most 128 MiB of HBM per device.

v0:
```python
import jax
import jax.numpy as jnp
from jax import lax
from jax.sharding import PartitionSpec as P

HEAD_DIM = 64
GRID_W = 64
VALUE_DIM = 128


norm_eps = 1e-06
rope_theta = 10000.0
block_limit = 1024


def rms_scale(matrix):
    return matrix * lax.rsqrt(jnp.mean(matrix * matrix, axis=-1, keepdims=True) + norm_eps)


def modulated(activations, shift, scale):
    return (rms_scale(activations.astype(jnp.float32)) * (1.0 + scale) + shift).astype(jnp.bfloat16)


def rotate(vectors, positions, grid_width):
    quarter = vectors.shape[-1] // 4
    inverse = rope_theta ** (-jnp.arange(quarter, dtype=jnp.float32) / quarter)
    grid_row = (positions // grid_width).astype(jnp.float32)
    grid_col = (positions % grid_width).astype(jnp.float32)
    angles = jnp.concatenate([grid_row[:, None] * inverse, grid_col[:, None] * inverse], axis=-1)
    cos_table = jnp.cos(angles)[:, None, :]
    sin_table = jnp.sin(angles)[:, None, :]
    former = vectors[..., : 2 * quarter]
    latter = vectors[..., 2 * quarter :]
    return jnp.concatenate(
        [former * cos_table - latter * sin_table, latter * cos_table + former * sin_table], axis=-1
    )


def absorb(carry_state, key_block, value_block, queries, head_count):
    maxima, totals, numerator = carry_state
    row_count = key_block.shape[0]
    scores = jnp.einsum(
        "mhqd,kmhd->mhqk",
        queries,
        key_block.reshape(row_count, 2, head_count, HEAD_DIM),
        preferred_element_type=jnp.float32,
    ) * HEAD_DIM ** (-0.5)
    new_maxima = jnp.maximum(maxima, jnp.max(scores, axis=-1))
    rescale = jnp.exp(maxima - new_maxima)
    weights = jnp.exp(scores - new_maxima[..., None])
    totals = totals * rescale + jnp.sum(weights, axis=-1)
    numerator = numerator * rescale[..., None] + jnp.einsum(
        "mhqk,khe->mhqe",
        weights.astype(jnp.bfloat16),
        value_block.reshape(row_count, head_count, VALUE_DIM),
        preferred_element_type=jnp.float32,
    )
    return (new_maxima, totals, numerator)


def absorb_all(carry_state, key_rows, value_rows, queries, head_count, shard_len):
    total_rows = key_rows.shape[0]
    shards = total_rows // shard_len
    shard_group = max(
        [
            candidate
            for candidate in range(1, shards + 1)
            if shards % candidate == 0 and candidate * shard_len <= block_limit
        ]
        + [1]
    )
    block_rows = shard_group * shard_len

    def absorb_block(block_index, inner_state):
        key_block = lax.dynamic_slice_in_dim(key_rows, block_index * block_rows, block_rows, 0)
        value_block = lax.dynamic_slice_in_dim(value_rows, block_index * block_rows, block_rows, 0)
        return absorb(inner_state, key_block, value_block, queries, head_count)

    return lax.fori_loop(0, total_rows // block_rows, absorb_block, carry_state)


def local(
    latent,
    context,
    cond_latent,
    cond_context,
    shift_weight,
    scale_weight,
    gate_weight,
    query_weight,
    key_weight,
    value_weight,
    out_weight,
    lambda_heads,
    out_gain,
):
    mod_rows = shift_weight.shape[0]
    conditions = jnp.stack([cond_latent, cond_context])
    conditions = jax.nn.silu(
        lax.dynamic_slice_in_dim(conditions, lax.axis_index("sp") * mod_rows, mod_rows, 1)
    )
    conditions = conditions.astype(jnp.bfloat16)
    partial_value = jnp.concatenate(
        [
            jnp.dot(conditions, shift_weight, preferred_element_type=jnp.float32),
            jnp.dot(conditions, scale_weight, preferred_element_type=jnp.float32),
            jnp.dot(conditions[:1], gate_weight, preferred_element_type=jnp.float32),
        ],
        axis=0,
    )
    summed_mod = lax.psum(partial_value, "sp")
    whole_mod = lax.all_gather(summed_mod, "tp", axis=1, tiled=True)
    hidden = modulated(latent, whole_mod[0], whole_mod[2])
    context_hidden = modulated(context, whole_mod[1], whole_mod[3])
    head_count = lambda_heads.shape[0]
    own_rows = latent.shape[0]
    tok_rows = own_rows * lax.axis_size("tp")
    row_offset = lax.axis_index("sp") * tok_rows
    piece_rows = lax.all_gather(hidden, "tp", axis=0, tiled=True)
    row_count = piece_rows.shape[0]
    positions = row_offset + jnp.arange(row_count, dtype=jnp.int32)

    def rotated(weight):
        product = jnp.concatenate(
            [
                jnp.dot(piece_rows, weight[0], preferred_element_type=jnp.float32),
                jnp.dot(piece_rows, weight[1], preferred_element_type=jnp.float32),
            ],
            axis=-1,
        )
        turned = rotate(product.reshape(row_count, 2 * head_count, HEAD_DIM), positions, GRID_W)
        return turned.reshape(row_count, 2 * head_count * HEAD_DIM).astype(jnp.bfloat16)

    values = jnp.dot(piece_rows, value_weight, preferred_element_type=jnp.float32).astype(
        jnp.bfloat16
    )
    projected = jnp.concatenate([rotated(query_weight), rotated(key_weight), values], axis=-1)
    key_width = 2 * head_count * HEAD_DIM
    queries = (
        projected[:, :key_width].reshape(tok_rows, 2, head_count, HEAD_DIM).transpose(1, 2, 0, 3)
    )
    latent_keys = projected[:, key_width : 2 * key_width]
    latent_values = projected[:, 2 * key_width :]
    context_keys = jnp.concatenate(
        [
            jnp.dot(context_hidden, key_weight[0], preferred_element_type=jnp.float32),
            jnp.dot(context_hidden, key_weight[1], preferred_element_type=jnp.float32),
        ],
        axis=-1,
    ).astype(jnp.bfloat16)
    context_values = jnp.dot(
        context_hidden, value_weight, preferred_element_type=jnp.float32
    ).astype(jnp.bfloat16)
    initial = (
        jnp.full((2, head_count, tok_rows), -jnp.inf, jnp.float32),
        jnp.zeros((2, head_count, tok_rows), jnp.float32),
        jnp.zeros((2, head_count, tok_rows, VALUE_DIM), jnp.float32),
    )
    context_dev = context_keys.shape[0]
    shard_len = tok_rows + context_dev
    value_width = context_values.shape[1]
    joined_keys = jnp.concatenate([latent_keys, context_keys], axis=0)
    joined_values = jnp.concatenate([latent_values, context_values], axis=0)
    context_total = context_dev * lax.axis_size("sp")
    pieces = (
        lax.all_gather(joined_keys, "sp", axis=0, tiled=True),
        lax.all_gather(joined_values, "sp", axis=0, tiled=True),
    )
    attention_state = initial
    shard_count = pieces[0].shape[0] // shard_len
    key_parts = pieces[0].reshape(shard_count, shard_len, key_width)
    value_parts = pieces[1].reshape(shard_count, shard_len, value_width)
    attention_state = absorb_all(
        attention_state,
        key_parts[:, :tok_rows].reshape(shard_count * tok_rows, key_width),
        value_parts[:, :tok_rows].reshape(shard_count * tok_rows, value_width),
        queries,
        head_count,
        tok_rows,
    )
    held_keys = key_parts[:, tok_rows:].reshape(shard_count * context_dev, key_width)
    held_values = value_parts[:, tok_rows:].reshape(shard_count * context_dev, value_width)
    folded, held_keys, held_values = (attention_state, held_keys, held_values)
    final = absorb_all(folded, held_keys, held_values, queries, head_count, context_total)
    totals = final[1]
    numerator = final[2]
    mixed = numerator[0] / totals[0][..., None] - lambda_heads[:, None, None] * (
        numerator[1] / totals[1][..., None]
    )
    normed = rms_scale(mixed) * out_gain.reshape(head_count, 1, VALUE_DIM)
    heads_out = (
        normed.transpose(1, 0, 2).reshape(tok_rows, head_count * VALUE_DIM).astype(jnp.bfloat16)
    )
    summed = lax.psum_scatter(
        jnp.dot(heads_out, out_weight, preferred_element_type=jnp.float32).astype(jnp.bfloat16),
        "tp",
        scatter_dimension=0,
        tiled=True,
    ).astype(jnp.float32)
    return (latent.astype(jnp.float32) + whole_mod[4] * summed).astype(jnp.bfloat16)


def solution(mesh):
    placed = (
        P(("sp", "tp"), None),
        P("sp", None),
        P(),
        P(),
        P("sp", "tp"),
        P("sp", "tp"),
        P("sp", "tp"),
        P(None, None, "tp"),
        P(None, None, "tp"),
        P(None, "tp"),
        P("tp", None),
        P("tp"),
        P("tp"),
    )
    return jax.shard_map(
        local, mesh=mesh, in_specs=placed, out_specs=P(("sp", "tp"), None), check_vma=False
    )
```

profile of v0, /device:TPU:0, one launch (start us, length us, event | category | flops | bytes accessed | tf_op | source)
XLA Modules:
  0.0 315.6 jit_solution(14840474781034838104)
XLA Ops:
  12.0 38.9 %psum.7 = f32[5,512]{1,0:T(8,128)S(1)} all-reduce(f32[5,512]{1,0:T(8,128)S(1)} %pad_maximum_fusion.8), channel_id=1, replica_groups=mesh['sp'=8,'tp'=4] {'sp'}, use_global_device_ids=true, to_apply=%region_0.1 | all-reduce | flops 2560 | bytes 20480 | tf_op jit(solution)/shard_map/psum | solution.py:111
  50.9 5.2 %all_gather.12 = f32[5,2048]{1,0:T(8,128)S(1)} all-gather(f32[5,512]{1,0:T(8,128)S(1)} %psum.7), channel_id=1, replica_groups=mesh['sp'=8,'tp'=4] {'tp'}, dimensions={1}, use_global_device_ids=true | all-gather | bytes 51200 | tf_op jit(solution)/shard_map/all_gather | solution.py:112
  56.7 1.9 fusion.35
  58.9 1.6 convolution_convert_fusion.3
  60.5 1.6 convolution_convert_fusion.4
  62.5 13.2 %all-gather.4.cloned.1.call-done = bf16[384,2048]{1,0:T(8,128)(2,1)} async-done(((bf16[96,2048]{1,0:T(8,128)(2,1)}), bf16[384,2048]{1,0:T(8,128)(2,1)}) %all-gather.4.cloned.1.call-update) | async-done | bytes 1572880 | tf_op jit(solution)/shard_map/all_gather | solution.py:119
  75.7 2.6 fusion.16
  78.3 2.3 fusion.18
  83.8 2.3 convolution_convert_fusion.2
  86.1 2.4 convolution_convert_fusion.1
  89.6 60.5 %all-gather.6.cloned.1.call-done = bf16[3584,512]{1,0:T(8,128)(2,1)} async-done(((bf16[448,512]{1,0:T(8,128)(2,1)}), bf16[3584,512]{1,0:T(8,128)(2,1)}) %all-gather.6.cloned.1.call-update) | async-done | bytes 3670032 | tf_op jit(solution)/shard_map/all_gather | solution.py:166
  151.2 3.8 %slice.98 = bf16[8,384,512]{2,1,0:T(8,128)(2,1)} slice(bf16[8,448,512]{2,1,0:T(8,128)(2,1)} %bitcast.129), slice={[0:8], [0:384], [0:512]} | slice | bytes 6291456 | tf_op jit(solution)/shard_map/slice | solution.py:175
  155.0 62.2 %all-gather.8.cloned.1.call-done = bf16[3584,512]{1,0:T(8,128)(2,1)} async-done(((bf16[448,512]{1,0:T(8,128)(2,1)}), bf16[3584,512]{1,0:T(8,128)(2,1)}) %all-gather.8.cloned.1.call-update) | async-done | bytes 3670032 | tf_op jit(solution)/shard_map/all_gather | solution.py:167
  218.4 3.7 %slice.101 = bf16[8,384,512]{2,1,0:T(8,128)(2,1)} slice(bf16[8,448,512]{2,1,0:T(8,128)(2,1)} %bitcast.131), slice={[0:8], [0:384], [0:512]} | slice | bytes 6291456 | tf_op jit(solution)/shard_map/slice | solution.py:176
  224.6 47.3 %while.5 = (s32[]{:T(128)}, f32[2,4,384]{2,1,0:T(4,128)S(1)}, f32[2,4,384]{2,1,0:T(4,128)}, f32[2,4,384,128]{2,3,0,1:T(8,128)}, bf16[3072,512]{1,0:T(8,128)(2,1)...) while((s32[]{:T(128)}, f32[2,4,384]{2,1,0:T(4,128)S(1)}, ...), condition=%wide.region_6.7_spmd.clone, body=%wide.region_3.6_spmd.clone.sunk | while | flops 921320448 | bytes 52605216 | solution.py:79
  224.6 2.4 constant_dynamic-slice_fusion.3
  229.6 2.6 bitcast_reduce_fusion.2
  232.2 1.9 fusion.91
  236.4 2.4 constant_dynamic-slice_fusion.3
  241.4 2.6 bitcast_reduce_fusion.2
  244.0 1.9 fusion.91
  248.2 2.4 constant_dynamic-slice_fusion.3
  253.2 2.6 bitcast_reduce_fusion.2
  255.8 1.9 fusion.91
  260.0 2.4 constant_dynamic-slice_fusion.3
  265.0 2.6 bitcast_reduce_fusion.2
  267.6 1.9 fusion.91
  271.9 2.4 multiply_reduce_fusion
  274.3 1.6 fusion.9
  278.1 2.2 convolution_convert_fusion
  280.3 26.9 %reduce-scatter.2.cloned.1.call-done = bf16[96,2048]{1,0:T(8,128)(2,1)} async-done(((bf16[384,2048]{1,0:T(8,128)(2,1)}), bf16[96,2048]{1,0:T(8,128)(2,1)}) %reduce-scatter.2.cloned.1.call-update) | async-done | bytes 393232 | tf_op jit(solution)/shard_map/reduce_scatter | solution.py:194
  307.2 1.9 fusion.36
  (135 shorter events, 37.3 us)
Async XLA Ops:
  6.5 271.6 %copy-start = (bf16[512,2048]{1,0:T(8,128)(2,1)S(1)}, bf16[512,2048]{1,0:T(8,128)(2,1)}, u32[]{:S(2)}) copy-start(bf16[512,2048]{1,0:T(8,128)(2,1)} %param.25) | copy-start | bytes 6291460
  6.5 52.2 %copy-start.7 = (bf16[64,2048]{1,0:T(8,128)(2,1)S(1)}, bf16[64,2048]{1,0:T(8,128)(2,1)}, u32[]{:S(2)}) copy-start(bf16[64,2048]{1,0:T(8,128)(2,1)} %param.16) | copy-start | bytes 786436
  6.5 69.2 %all-gather.4.cloned.1.call-start = ((), (), s32[]{:S(2)}) async-start(), calls=%async_computation.1 | async-start | bytes 1966080 | tf_op jit(solution)/shard_map/all_gather | solution.py:119
  58.7 91.5 %all-gather.6.cloned.1.call-start = ((), (), s32[]{:S(2)}) async-start(), calls=%async_computation.2 | async-start | bytes 4128768 | tf_op jit(solution)/shard_map/all_gather | solution.py:166
  75.7 2.6 copy-start.14
  78.3 2.4 copy-start.15
  78.3 2.5 copy-start.16
  83.8 133.5 %all-gather.8.cloned.1.call-start = ((), (), s32[]{:S(2)}) async-start(), calls=%async_computation.3 | async-start | bytes 4128768 | tf_op jit(solution)/shard_map/all_gather | solution.py:167
  83.8 2.3 copy-start.6
  89.3 217.9 %reduce-scatter.2.cloned.1.call-start = ((), (), s32[]{:S(2)}) async-start(), calls=%async_computation.4 | async-start | bytes 1966080 | tf_op jit(solution)/shard_map/reduce_scatter | solution.py:194
  232.2 1.9 copy-start.8
  232.2 1.9 copy-start.1
  234.1 1.2 copy-start.9
  235.3 1.1 copy-start.2
  244.0 1.9 copy-start.8
  244.0 1.9 copy-start.1
  245.9 1.2 copy-start.9
  247.1 1.1 copy-start.2
  255.8 1.9 copy-start.8
  255.8 1.9 copy-start.1
  257.7 1.2 copy-start.9
  258.9 1.1 copy-start.2
  267.6 1.9 copy-start.8
  267.6 1.9 copy-start.1
  269.5 1.2 copy-start.9
  270.7 1.1 copy-start.2
  274.3 1.7 copy-start.10
  274.3 1.7 copy-start.3
  274.3 1.7 copy-start.5
  276.0 1.2 copy-start.13
  278.1 29.1 %copy-start.4 = (bf16[96,2048]{1,0:T(8,128)(2,1)S(1)}, bf16[96,2048]{1,0:T(8,128)(2,1)}, u32[]{:S(2)}) copy-start(bf16[96,2048]{1,0:T(8,128)(2,1)} %param.15) | copy-start | bytes 1179652
  278.1 29.1 %copy-start.11 = (f32[1,2048]{1,0:T(1,128)S(1)}, f32[1,2048]{1,0:T(1,128)}, u32[]{:S(2)}) copy-start(f32[1,2048]{1,0:T(1,128)} %get-tuple-element.237) | copy-start | bytes 24580
  (1 other events, 0.7 us)
Sparse Core Ops, SparseCore 0:
  58.8 16.8 all-gather.3
  83.9 66.2 all-gather.5
  152.3 64.9 all-gather.7
  280.5 26.7 reduce-scatter.1
where the time goes:
time: 317 us; the launch traced here: 316 us
  waiting for transfers between devices  163 us (51%)
  blocking collectives  44.1 us (14%)
  local copies, waits for them, and re-layouts  38.4 us (12%)
  matrix products  38.1 us (12%)
  other arithmetic  17.9 us (6%)
  between operations  13.5 us (4%)
    all_gather x1, waiting for transfers between devices, local(): lax.all_gather(joined_values, 'sp', axis=0, tiled=True)  62.2 us
    all_gather x1, waiting for transfers between devices, local(): lax.all_gather(joined_keys, 'sp', axis=0, tiled=True)  60.5 us
    psum x1, blocking collectives, local(): summed_mod = lax.psum(partial_value, 'sp')  38.9 us
    reduce_scatter x1, waiting for transfers between devices, local(): lax.psum_scatter(jnp.dot(heads_out, out_weight, preferred_element_type=jn...  26.9 us
    dynamic_slice x8, local copies, waits for them, and re-layouts, absorb_block(): lax.dynamic_slice_in_dim(value_rows, block_index * block_rows, block_rows...  15 us
    all_gather x1, waiting for transfers between devices, local(): piece_rows = lax.all_gather(hidden, 'tp', axis=0, tiled=True)  13.2 us
    dot_general x5, matrix products, absorb(): jnp.einsum('mhqd,kmhd->mhqk', queries, key_block.reshape(row_count, 2, he...  12.7 us
    convert_element_type x5, other arithmetic, absorb(): weights.astype(jnp.bfloat16)  9.04 us
  transfers between devices with their start and end apart: 4, of which 4 were waited for; matrix products, arithmetic and copies ran while one was open for 4% of the time, Pallas kernels for 0%

commit v1 on v0

v1 whole, which is shorter than its diff:
```python
import functools

import jax
import jax.numpy as jnp
from jax import lax
from jax.experimental import pallas as pl
from jax.experimental.pallas import tpu as pltpu
from jax.sharding import PartitionSpec as P

HEAD_DIM = 64
GRID_W = 64
VALUE_DIM = 128
LANES = 128

norm_eps = 1e-06
rope_theta = 10000.0
f32 = jnp.float32
bf16 = jnp.bfloat16
MESH = pl.DeviceIdType.MESH


def pick(total, limit, unit):
    best = unit
    for size in range(unit, limit + 1, unit):
        if total % size == 0:
            best = size
    return best


def body(
    n_sp,
    n_tp,
    lat,
    ctx,
    cond_l,
    cond_c,
    shift_w,
    scale_w,
    gate_w,
    lane_table,
    lam,
    gain,
    wq_hbm,
    wk_hbm,
    wv_hbm,
    wo_hbm,
    out,
    wq,
    wk,
    wv,
    wo,
    mod_part,
    mod_recv,
    mod_all,
    raw,
    hidden,
    cos_t,
    sin_t,
    q_send,
    kv_send,
    kvc_send,
    q_buf,
    kv_buf,
    scores,
    o_send,
    heads,
    pair_send,
    pair_recv,
    fin_send,
    fin_recv,
    own_sum,
    w_sem,
    loc_sem,
    mod1_s,
    mod1_r,
    mod2_s,
    mod2_r,
    raw_s,
    raw_r,
    fwd_s,
    fwd_r,
    q_s,
    q_r,
    kv_s,
    kv_r,
    kvc_s,
    kvc_r,
    rel_s,
    rel_r,
    relc_s,
    relc_r,
    o_s,
    o_r,
    pair_s,
    pair_r,
    fin_s,
    fin_r,
):
    own, width = lat.shape
    ctx_rows = ctx.shape[0]
    tok = own * n_tp
    mod_cols = shift_w.shape[1]
    groups = q_send.shape[0]
    ranks = n_sp // groups
    chips = n_tp // 2
    sp_i = lax.axis_index("sp")
    tp_i = lax.axis_index("tp")
    g_i = sp_i // ranks
    r_i = sp_i % ranks
    chip_i = tp_i // 2
    core_i = tp_i % 2
    partner = chip_i * 2 + (1 - core_i)
    pending = []

    def send(src, dst, s_sem, r_sem, **where):
        copy = pltpu.make_async_remote_copy(
            src_ref=src, dst_ref=dst, send_sem=s_sem, recv_sem=r_sem,
            device_id=where, device_id_type=MESH,
        )
        copy.start()
        pending.append(copy)

    def arrived(ref, s_sem, r_sem, **where):
        pltpu.make_async_remote_copy(
            src_ref=ref, dst_ref=ref, send_sem=s_sem, recv_sem=r_sem,
            device_id=where, device_id_type=MESH,
        ).wait_recv()

    loads = [
        pltpu.make_async_copy(src, dst, w_sem.at[i])
        for i, (src, dst) in enumerate(
            ((wk_hbm, wk), (wv_hbm, wv), (wq_hbm, wq), (wo_hbm, wo))
        )
    ]
    for load in loads:
        load.start()

    barrier = pltpu.get_barrier_semaphore()
    for k in range(1, n_sp):
        pl.semaphore_signal(
            barrier, inc=1, device_id={"sp": (sp_i + k) % n_sp}, device_id_type=MESH
        )
    for k in range(1, n_tp):
        pl.semaphore_signal(
            barrier, inc=1, device_id={"tp": (tp_i + k) % n_tp}, device_id_type=MESH
        )

    def silu(v):
        return (v / (1.0 + jnp.exp(-v))).astype(bf16).astype(f32)

    c0 = silu(cond_l[sp_i])
    c1 = silu(cond_c[sp_i])
    row = lax.broadcasted_iota(jnp.int32, (8, c0.shape[-1]), 0)

    def placed_rows(at0, at1):
        zero = jnp.zeros(row.shape, f32)
        rows = jnp.where(row == at0, jnp.broadcast_to(c0, row.shape), zero)
        if at1 is not None:
            rows = jnp.where(row == at1, jnp.broadcast_to(c1, row.shape), rows)
        return rows.astype(bf16)

    mod_part[...] = (
        jnp.dot(placed_rows(0, 1), shift_w[...], preferred_element_type=f32)
        + jnp.dot(placed_rows(2, 3), scale_w[...], preferred_element_type=f32)
        + jnp.dot(placed_rows(4, None), gate_w[...], preferred_element_type=f32)
    )
    pl.semaphore_wait(barrier, n_sp + n_tp - 2)

    for k in range(1, n_sp):
        send(
            mod_part, mod_recv.at[sp_i], mod1_s.at[k], mod1_r.at[sp_i], sp=(sp_i + k) % n_sp
        )
    for k in range(1, chips):
        send(
            lat, raw.at[tp_i], raw_s.at[k], raw_r.at[chip_i],
            tp=((chip_i + k) % chips) * 2 + core_i,
        )
    send(lat, raw.at[tp_i], fwd_s.at[0], fwd_r.at[chip_i], tp=partner)
    raw[tp_i] = lat[...]
    mod_recv[sp_i] = mod_part[...]

    tok_row = lax.broadcasted_iota(jnp.int32, (tok, LANES), 0) + sp_i * tok
    grid_row = (tok_row // GRID_W).astype(f32)
    grid_col = (tok_row % GRID_W).astype(f32)
    angles = grid_row * lane_table[0:1, :] + grid_col * lane_table[1:2, :]
    cos_t[...] = jnp.cos(angles)
    sin_t[...] = jnp.sin(angles) * lane_table[2:3, :]

    for k in range(1, n_sp):
        src = (sp_i + n_sp - k) % n_sp
        arrived(mod_recv.at[src], mod1_s.at[k], mod1_r.at[src], sp=src)
    total = mod_recv[0]
    for s in range(1, n_sp):
        total = total + mod_recv[s]
    mod_part2 = mod_all.at[tp_i]
    mod_part2[...] = total
    for k in range(1, n_tp):
        send(
            mod_part2, mod_all.at[tp_i], mod2_s.at[k], mod2_r.at[tp_i], tp=(tp_i + k) % n_tp
        )
    for k in range(1, chips):
        src_chip = (chip_i + chips - k) % chips
        slot = src_chip * 2 + core_i
        arrived(raw.at[slot], raw_s.at[k], raw_r.at[src_chip], tp=slot)
        send(raw.at[slot], raw.at[slot], fwd_s.at[k], fwd_r.at[src_chip], tp=partner)
    for k in range(1, n_tp):
        src = (tp_i + n_tp - k) % n_tp
        arrived(mod_all.at[src], mod2_s.at[k], mod2_r.at[src], tp=src)

    def modulate(x, which, start):
        rows = x.shape[0]
        factor = lax.rsqrt(jnp.mean(x * x, axis=-1, keepdims=True) + norm_eps)
        for t in range(n_tp):
            cols = slice(t * mod_cols, (t + 1) * mod_cols)
            shift = mod_all[t, which : which + 1, :]
            scale = mod_all[t, which + 2 : which + 3, :]
            hidden[start : start + rows, cols] = (
                (x[:, cols] * factor) * (1.0 + scale) + shift
            ).astype(bf16)

    modulate(ctx[...].astype(f32), 1, tok)
    for k in range(chips):
        src_chip = (chip_i + chips - k) % chips
        slot = src_chip * 2 + (1 - core_i)
        arrived(raw.at[slot], fwd_s.at[k], fwd_r.at[src_chip], tp=partner)
    for t in range(n_tp):
        modulate(raw[t].astype(f32), 0, t * own)

    lane = lax.broadcasted_iota(jnp.int32, (tok, LANES), 1)
    first_quarter = lane % HEAD_DIM < HEAD_DIM // 2
    ctx_half = lax.broadcasted_iota(jnp.int32, (ctx_rows, LANES), 1) < HEAD_DIM

    def rope(u):
        swapped = jnp.where(
            first_quarter,
            pltpu.roll(u, LANES - HEAD_DIM // 2, 1),
            pltpu.roll(u, HEAD_DIM // 2, 1),
        )
        return u * cos_t[...] + swapped * sin_t[...]

    def pair_up(a, b, low):
        return (
            jnp.where(low, a, pltpu.roll(b, HEAD_DIM, 1)).astype(bf16),
            jnp.where(low, pltpu.roll(a, HEAD_DIM, 1), b).astype(bf16),
        )

    low_half = lane < HEAD_DIM
    loads[0].wait()
    keys = [jnp.dot(hidden[...], wk[m], preferred_element_type=f32) for m in (0, 1)]
    for p in range(groups // 2):
        slab = slice(p * LANES, (p + 1) * LANES)
        a, b = pair_up(rope(keys[0][:tok, slab]), rope(keys[1][:tok, slab]), low_half)
        kv_send[2 * p, :, :LANES] = a
        kv_send[2 * p + 1, :, :LANES] = b
        a, b = pair_up(keys[0][tok:, slab], keys[1][tok:, slab], ctx_half)
        kvc_send[2 * p, :, :LANES] = a
        kvc_send[2 * p + 1, :, :LANES] = b
    loads[1].wait()
    vals = jnp.dot(hidden[...], wv[...], preferred_element_type=f32).astype(bf16)
    for j in range(groups):
        slab = slice(j * LANES, (j + 1) * LANES)
        kv_send[j, :, LANES:] = vals[:tok, slab]
        kvc_send[j, :, LANES:] = vals[tok:, slab]

    def lat_slot(s):
        return kv_buf.at[pl.ds(pl.multiple_of(s * tok, 16), tok)]

    def ctx_slot(s):
        return kv_buf.at[pl.ds(pl.multiple_of(n_sp * tok + s * ctx_rows, 16), ctx_rows)]

    order = list(range(1, groups))
    for k in order:
        g = (g_i + k) % groups
        send(kv_send.at[g], lat_slot(sp_i), kv_s.at[k], kv_r.at[g_i], sp=g * ranks + r_i)
        send(kvc_send.at[g], ctx_slot(sp_i), kvc_s.at[k], kvc_r.at[g_i], sp=g * ranks + r_i)
    for e in range(1, ranks):
        to = g_i * ranks + (r_i + e) % ranks
        send(kv_send.at[g_i], lat_slot(sp_i), rel_s.at[0, e], rel_r.at[g_i, r_i], sp=to)
        send(kvc_send.at[g_i], ctx_slot(sp_i), relc_s.at[0, e], relc_r.at[g_i, r_i], sp=to)
    local = [
        pltpu.make_async_copy(kv_send.at[g_i], lat_slot(sp_i), loc_sem.at[0]),
        pltpu.make_async_copy(kvc_send.at[g_i], ctx_slot(sp_i), loc_sem.at[1]),
    ]
    for copy in local:
        copy.start()

    loads[2].wait()
    queries = [jnp.dot(hidden[:tok, :], wq[m], preferred_element_type=f32) for m in (0, 1)]
    for p in range(groups // 2):
        slab = slice(p * LANES, (p + 1) * LANES)
        a, b = pair_up(rope(queries[0][:, slab]), rope(queries[1][:, slab]), low_half)
        q_send[2 * p] = a
        q_send[2 * p + 1] = b
    for k in order:
        g = (g_i + k) % groups
        send(q_send.at[g], q_buf.at[g_i], q_s.at[k], q_r.at[g_i], sp=g * ranks + r_i)
    q_local = pltpu.make_async_copy(q_send.at[g_i], q_buf.at[g_i], loc_sem.at[2])
    q_local.start()

    for k in order:
        g = (g_i + groups - k) % groups
        s = g * ranks + r_i
        arrived(lat_slot(s), kv_s.at[k], kv_r.at[g], sp=s)
        for e in range(1, ranks):
            to = g_i * ranks + (r_i + e) % ranks
            send(lat_slot(s), lat_slot(s), rel_s.at[k, e], rel_r.at[g, r_i], sp=to)
        arrived(ctx_slot(s), kvc_s.at[k], kvc_r.at[g], sp=s)
        for e in range(1, ranks):
            to = g_i * ranks + (r_i + e) % ranks
            send(ctx_slot(s), ctx_slot(s), relc_s.at[k, e], relc_r.at[g, r_i], sp=to)
    for copy in local:
        copy.wait()
    q_local.wait()
    for k in order:
        g = (g_i + groups - k) % groups
        arrived(q_buf.at[g], q_s.at[k], q_r.at[g], sp=g * ranks + r_i)
    for e in range(1, ranks):
        r = (r_i + ranks - e) % ranks
        for k in range(groups):
            g = (g_i + groups - k) % groups
            s = g * ranks + r
            arrived(lat_slot(s), rel_s.at[k, e], rel_r.at[g, r], sp=g_i * ranks + r)
            arrived(ctx_slot(s), relc_s.at[k, e], relc_r.at[g, r], sp=g_i * ranks + r)

    key_total = kv_buf.shape[0]
    q_tile = scores.shape[0] // 2
    block = pick(key_total, 512, LANES)
    coef = HEAD_DIM ** (-0.5) * 1.4426950408889634
    q_low = lax.broadcasted_iota(jnp.int32, (q_tile, LANES), 1) < HEAD_DIM
    head_lam = lam[g_i]
    head_gain = gain[g_i]

    def attend(g, start):
        q = q_buf[g, pl.ds(start, q_tile), :]
        zero = jnp.zeros_like(q)
        q2 = jnp.concatenate([jnp.where(q_low, q, zero), jnp.where(q_low, zero, q)], axis=0)
        peak = None
        for b in range(key_total // block):
            rows = slice(b * block, (b + 1) * block)
            s = lax.dot_general(
                q2, kv_buf[rows, :LANES], (((1,), (1,)), ((), ())), preferred_element_type=f32
            )
            scores[:, rows] = s
            for c in range(block // LANES):
                piece = s[:, c * LANES : (c + 1) * LANES]
                peak = piece if peak is None else jnp.maximum(peak, piece)
        top = jnp.max(peak, axis=-1, keepdims=True) * coef
        sums = None
        acc = None
        for b in range(key_total // block):
            rows = slice(b * block, (b + 1) * block)
            w = jnp.exp2(scores[:, rows] * coef - top)
            for c in range(block // LANES):
                piece = w[:, c * LANES : (c + 1) * LANES]
                sums = piece if sums is None else sums + piece
            part = jnp.dot(w.astype(bf16), kv_buf[rows, LANES:], preferred_element_type=f32)
            acc = part if acc is None else acc + part
        mean_v = acc / jnp.sum(sums, axis=-1, keepdims=True)
        mixed = mean_v[:q_tile] - head_lam * mean_v[q_tile:]
        factor = lax.rsqrt(jnp.mean(mixed * mixed, axis=-1, keepdims=True) + norm_eps)
        o_send[g, pl.ds(start, q_tile), :] = (mixed * factor * head_gain).astype(bf16)

    def o_copy(k):
        g = (g_i + 1 + k) % groups
        return pltpu.make_async_remote_copy(
            src_ref=o_send.at[g], dst_ref=heads.at[g_i], send_sem=o_s.at[k],
            recv_sem=o_r.at[g_i], device_id={"sp": g * ranks + r_i}, device_id_type=MESH,
        )

    @pl.loop(0, groups)
    def _(k):
        g = (g_i + 1 + k) % groups

        @pl.loop(0, tok // q_tile)
        def _(i):
            attend(g, pl.multiple_of(i * q_tile, q_tile))

        @pl.when(k < groups - 1)
        def _():
            o_copy(k).start()

    heads[g_i] = o_send[g_i]
    loads[3].wait()
    for k in range(groups - 1):
        src = (g_i + groups - 1 - k) % groups
        arrived(heads.at[src], o_s.at[k], o_r.at[src], sp=src * ranks + r_i)

    def term(chunk):
        start = pl.multiple_of(chunk * own, 16)
        left = jnp.concatenate(
            [heads[h, pl.ds(start, own), :] for h in range(groups)], axis=-1
        )
        return jnp.dot(left, wo[...], preferred_element_type=f32).astype(bf16)

    for k in range(chips):
        chip = (chip_i + 1 + k) % chips
        pair_send[k] = term(chip * 2 + (1 - core_i))
        send(pair_send.at[k], pair_recv.at[k], pair_s.at[k], pair_r.at[k], tp=partner)
    for k in range(chips):
        chip = (chip_i + 1 + k) % chips
        mine = term(chip * 2 + core_i).astype(f32)
        arrived(pair_recv.at[k], pair_s.at[k], pair_r.at[k], tp=partner)
        both = mine + pair_recv[k].astype(f32)
        if k < chips - 1:
            fin_send[k] = both.astype(bf16)
            send(
                fin_send.at[k], fin_recv.at[k], fin_s.at[k], fin_r.at[k], tp=chip * 2 + core_i
            )
        else:
            own_sum[...] = both
    for k in range(chips - 1):
        src_chip = (chip_i + chips - 1 - k) % chips
        arrived(fin_recv.at[k], fin_s.at[k], fin_r.at[k], tp=src_chip * 2 + core_i)
    for t in range(n_tp):
        cols = slice(t * mod_cols, (t + 1) * mod_cols)
        summed = own_sum[:, cols]
        for k in range(chips - 1):
            summed = summed + fin_recv[k, :, cols].astype(f32)
        out[:, cols] = (
            lat[:, cols].astype(f32) + mod_all[t, 4:5, :] * summed
        ).astype(bf16)
    for copy in pending:
        copy.wait_send()
    for k in range(groups - 1):
        o_copy(k).wait_send()


def local(
    n_sp,
    n_tp,
    latent,
    context,
    cond_latent,
    cond_context,
    shift_weight,
    scale_weight,
    gate_weight,
    query_weight,
    key_weight,
    value_weight,
    out_weight,
    lambda_heads,
    out_gain,
):
    own, width = latent.shape
    ctx_rows = context.shape[0]
    tok = own * n_tp
    groups = lambda_heads.shape[0]
    ranks = n_sp // groups
    chips = n_tp // 2
    mod_rows, mod_cols = shift_weight.shape
    keys = n_sp * (tok + ctx_rows)
    q_tile = pick(tok, 128, 16)

    quarter = HEAD_DIM // 4
    inverse = rope_theta ** (-jnp.arange(quarter, dtype=f32) / quarter)
    zeros = jnp.zeros((quarter,), f32)
    repeat = LANES // (2 * quarter)
    half = jnp.ones((2 * quarter,), f32)
    lane_table = jnp.stack(
        [
            jnp.tile(jnp.concatenate([inverse, zeros]), repeat),
            jnp.tile(jnp.concatenate([zeros, inverse]), repeat),
            jnp.tile(jnp.concatenate([-half, half]), repeat // 2),
        ]
        + [jnp.zeros((LANES,), f32)] * 5
    )
    lam = jnp.broadcast_to(lambda_heads[:, None, None], (groups, 1, LANES))
    gain = out_gain.reshape(groups, 1, VALUE_DIM)
    vmem = pl.BlockSpec(memory_space=pltpu.VMEM)
    hbm = pl.BlockSpec(memory_space=pl.ANY)
    dma = pltpu.SemaphoreType.DMA
    scratch = [
        pltpu.VMEM(query_weight.shape, bf16),
        pltpu.VMEM(key_weight.shape, bf16),
        pltpu.VMEM(value_weight.shape, bf16),
        pltpu.VMEM(out_weight.shape, bf16),
        pltpu.VMEM((8, mod_cols), f32),
        pltpu.VMEM((n_sp, 8, mod_cols), f32),
        pltpu.VMEM((n_tp, 8, mod_cols), f32),
        pltpu.VMEM((n_tp, own, width), bf16),
        pltpu.VMEM((tok + ctx_rows, width), bf16),
        pltpu.VMEM((tok, LANES), f32),
        pltpu.VMEM((tok, LANES), f32),
        pltpu.VMEM((groups, tok, LANES), bf16),
        pltpu.VMEM((groups, tok, 2 * LANES), bf16),
        pltpu.VMEM((groups, ctx_rows, 2 * LANES), bf16),
        pltpu.VMEM((groups, tok, LANES), bf16),
        pltpu.VMEM((keys, 2 * LANES), bf16),
        pltpu.VMEM((2 * q_tile, keys), f32),
        pltpu.VMEM((groups, tok, LANES), bf16),
        pltpu.VMEM((groups, tok, LANES), bf16),
        pltpu.VMEM((chips, own, width), bf16),
        pltpu.VMEM((chips, own, width), bf16),
        pltpu.VMEM((max(chips - 1, 1), own, width), bf16),
        pltpu.VMEM((max(chips - 1, 1), own, width), bf16),
        pltpu.VMEM((own, width), f32),
        dma((4,)),
        dma((3,)),
        dma((n_sp,)),
        dma((n_sp,)),
        dma((n_tp,)),
        dma((n_tp,)),
        dma((chips,)),
        dma((chips,)),
        dma((chips,)),
        dma((chips,)),
        dma((groups,)),
        dma((groups,)),
        dma((groups,)),
        dma((groups,)),
        dma((groups,)),
        dma((groups,)),
        dma((groups, ranks)),
        dma((groups, ranks)),
        dma((groups, ranks)),
        dma((groups, ranks)),
        dma((groups,)),
        dma((groups,)),
        dma((chips,)),
        dma((chips,)),
        dma((chips,)),
        dma((chips,)),
    ]
    return pl.pallas_call(
        functools.partial(body, n_sp, n_tp),
        out_shape=jax.ShapeDtypeStruct((own, width), bf16),
        in_specs=[vmem] * 10 + [hbm] * 4,
        out_specs=vmem,
        scratch_shapes=scratch,
        compiler_params=pltpu.CompilerParams(
            collective_id=0, has_side_effects=True, vmem_limit_bytes=60 * 1024 * 1024
        ),
        name="diff_attention",
    )(
        latent,
        context,
        cond_latent.reshape(n_sp, 1, mod_rows),
        cond_context.reshape(n_sp, 1, mod_rows),
        shift_weight,
        scale_weight,
        gate_weight,
        lane_table,
        lam,
        gain,
        query_weight,
        key_weight,
        value_weight,
        out_weight,
    )


def solution(mesh):
    placed = (
        P(("sp", "tp"), None),
        P("sp", None),
        P(),
        P(),
        P("sp", "tp"),
        P("sp", "tp"),
        P("sp", "tp"),
        P(None, None, "tp"),
        P(None, None, "tp"),
        P(None, "tp"),
        P("tp", None),
        P("tp"),
        P("tp"),
    )
    return jax.shard_map(
        functools.partial(local, mesh.shape["sp"], mesh.shape["tp"]),
        mesh=mesh,
        in_specs=placed,
        out_specs=P(("sp", "tp"), None),
        check_vma=False,
    )
```

time: 317 us -> 96.3 us (0.30)
  the two profiles are of different devices: /device:TPU:0 before, /device:TPU:24 now
where the time goes in v1:
time: 96.3 us; the launch traced here: 96.1 us
  Pallas kernels  91.4 us (95%)
  local copies, waits for them, and re-layouts  4.66 us (5%)
    pallas_call x1, Pallas kernels, local(): pl.pallas_call(functools.partial(body, n_sp, n_tp), out_shape=jax.ShapeDt...  91.4 us

profile of v1, /device:TPU:24, one launch (start us, length us, event | category | flops | bytes accessed | tf_op | source)
XLA Modules:
  0.0 96.1 jit_solution(2174903310078592527)
XLA Ops:
  0.0 0.1 fusion
  0.1 0.7 tile.8
  0.7 0.1 stack_tile.11
  0.8 0.1 stack_tile.10
  0.9 0.1 stack_tile.9
  1.0 1.3 %broadcast_in_dim.2.lam = f32[4,1,128]{2,1,0:T(1,128)} broadcast(f32[4]{0:T(128)} %param.24), dimensions={0} | broadcast | bytes 2064 | tf_op jit(solution)/shard_map/broadcast_in_dim | solution.py:468
  2.3 0.6 stack.7.lane_table
  2.9 91.4 %diff_attention.1 = bf16[96,2048]{1,0:T(8,128)(2,1)} custom-call(bf16[96,2048]{1,0:T(8,128)(2,1)} %lat.1, bf16[64,2048]{1,0:T(8,128)(2,1)} %ctx.1, f32[8,1,256]{2,1,0:T(1,128)} %bitcast.3, f32[8,1,256]{2,1,0:T(1,128)} %bitcast.4, bf16[256,512]{1,0:T(8,128)(2,1)} %shift_w.1, bf16[256,512]{1,0:T(8,128)(2,1)} %scale_w.1, bf16[256,512]{1,0:T(8,128)(2,1)} %gate_w.1, ...), custom_call_target="tpu_custom_call" | custom-call | tf_op jit(solution)/shard_map/diff_attention/pallas_call | solution.py:525
  94.3 1.8 %copy.15 = bf16[96,2048]{1,0:T(8,128)(2,1)} copy(bf16[96,2048]{1,0:T(8,128)(2,1)} %diff_attention.1) | data formatting | bytes 786432
  (5 shorter events, 0.0 us)

commit v2 on v1

v2 whole, which is shorter than its diff:
```python
import functools

import jax
import jax.numpy as jnp
import numpy as np
from jax import lax
from jax.experimental import pallas as pl
from jax.experimental.pallas import tpu as pltpu
from jax.sharding import PartitionSpec as P

HEAD_DIM = 64
GRID_W = 64
VALUE_DIM = 128
LANES = 128

norm_eps = 1e-06
rope_theta = 10000.0
f32 = jnp.float32
bf16 = jnp.bfloat16
MESH = pl.DeviceIdType.MESH


def pick(total, limit, unit):
    best = unit
    for size in range(unit, limit + 1, unit):
        if total % size == 0:
            best = size
    return best


def body(
    n_sp,
    n_tp,
    lat,
    ctx,
    cond_l,
    cond_c,
    shift_w,
    scale_w,
    gate_w,
    lane_table,
    lam,
    gain,
    wq_hbm,
    wk_hbm,
    wv_hbm,
    wo_hbm,
    out,
    wq,
    wk,
    wv,
    wo,
    mod_part,
    mod_recv,
    mod_all,
    raw,
    hidden,
    cos_t,
    sin_t,
    q_send,
    kv_send,
    kvc_send,
    q_buf,
    kv_buf,
    scores,
    o_send,
    heads,
    pair_send,
    pair_recv,
    fin_send,
    fin_recv,
    own_sum,
    w_sem,
    loc_sem,
    mod1_s,
    mod1_r,
    mod2_s,
    mod2_r,
    raw_s,
    raw_r,
    fwd_s,
    fwd_r,
    q_s,
    q_r,
    kv_s,
    kv_r,
    kvc_s,
    kvc_r,
    rel_s,
    rel_r,
    relc_s,
    relc_r,
    o_s,
    o_r,
    pair_s,
    pair_r,
    fin_s,
    fin_r,
):
    own, width = lat.shape
    ctx_rows = ctx.shape[0]
    tok = own * n_tp
    mod_cols = shift_w.shape[1]
    groups = q_send.shape[0]
    ranks = n_sp // groups
    chips = n_tp // 2
    sp_i = lax.axis_index("sp")
    tp_i = lax.axis_index("tp")
    g_i = sp_i // ranks
    r_i = sp_i % ranks
    chip_i = tp_i // 2
    core_i = tp_i % 2
    partner = chip_i * 2 + (1 - core_i)
    pending = []

    def send(src, dst, s_sem, r_sem, **where):
        copy = pltpu.make_async_remote_copy(
            src_ref=src, dst_ref=dst, send_sem=s_sem, recv_sem=r_sem,
            device_id=where, device_id_type=MESH,
        )
        copy.start()
        pending.append(copy)

    def arrived(ref, s_sem, r_sem, **where):
        pltpu.make_async_remote_copy(
            src_ref=ref, dst_ref=ref, send_sem=s_sem, recv_sem=r_sem,
            device_id=where, device_id_type=MESH,
        ).wait_recv()

    loads = [
        pltpu.make_async_copy(src, dst, w_sem.at[i])
        for i, (src, dst) in enumerate(
            ((wk_hbm, wk), (wv_hbm, wv), (wq_hbm, wq), (wo_hbm, wo))
        )
    ]
    for load in loads:
        load.start()

    barrier = pltpu.get_barrier_semaphore()
    for k in range(1, n_sp):
        pl.semaphore_signal(
            barrier, inc=1, device_id={"sp": (sp_i + k) % n_sp}, device_id_type=MESH
        )
    for k in range(1, n_tp):
        pl.semaphore_signal(
            barrier, inc=1, device_id={"tp": (tp_i + k) % n_tp}, device_id_type=MESH
        )

    def silu(v):
        return (v / (1.0 + jnp.exp(-v))).astype(bf16).astype(f32)

    c0 = silu(cond_l[sp_i])
    c1 = silu(cond_c[sp_i])
    row = lax.broadcasted_iota(jnp.int32, (8, c0.shape[-1]), 0)

    def placed_rows(at0, at1):
        zero = jnp.zeros(row.shape, f32)
        rows = jnp.where(row == at0, jnp.broadcast_to(c0, row.shape), zero)
        if at1 is not None:
            rows = jnp.where(row == at1, jnp.broadcast_to(c1, row.shape), rows)
        return rows.astype(bf16)

    mod_part[...] = (
        jnp.dot(placed_rows(0, 1), shift_w[...], preferred_element_type=f32)
        + jnp.dot(placed_rows(2, 3), scale_w[...], preferred_element_type=f32)
        + jnp.dot(placed_rows(4, None), gate_w[...], preferred_element_type=f32)
    )
    pl.semaphore_wait(barrier, n_sp + n_tp - 2)

    for k in range(1, n_sp):
        send(
            mod_part, mod_recv.at[sp_i], mod1_s.at[k], mod1_r.at[sp_i], sp=(sp_i + k) % n_sp
        )
    pieces = raw_s.shape[1]
    piece_rows = own // pieces

    def raw_piece(slot, i):
        return raw.at[slot, pl.ds(i * piece_rows, piece_rows)]

    def send_raw(i):
        for k in range(1, chips):
            send(
                lat.at[pl.ds(i * piece_rows, piece_rows)], raw_piece(tp_i, i),
                raw_s.at[k, i], raw_r.at[chip_i, i],
                tp=((chip_i + k) % chips) * 2 + core_i,
            )

    def relay_raw(i):
        for k in range(1, chips):
            src_chip = (chip_i + chips - k) % chips
            slot = src_chip * 2 + core_i
            arrived(raw_piece(slot, i), raw_s.at[k, i], raw_r.at[src_chip, i], tp=slot)
            send(
                raw_piece(slot, i), raw_piece(slot, i), fwd_s.at[k, i], fwd_r.at[src_chip, i],
                tp=partner,
            )

    early = max(pieces - 1, 1)
    for i in range(early):
        send_raw(i)
    send(lat, raw.at[tp_i], fwd_s.at[0, 0], fwd_r.at[chip_i, 0], tp=partner)
    raw[tp_i] = lat[...]
    mod_recv[sp_i] = mod_part[...]

    tok_row = lax.broadcasted_iota(jnp.int32, (tok, LANES), 0) + sp_i * tok
    grid_row = (tok_row // GRID_W).astype(f32)
    grid_col = (tok_row % GRID_W).astype(f32)
    angles = grid_row * lane_table[0:1, :] + grid_col * lane_table[1:2, :]
    cos_t[...] = jnp.cos(angles)
    sin_t[...] = jnp.sin(angles) * lane_table[2:3, :]

    for k in range(1, n_sp):
        src = (sp_i + n_sp - k) % n_sp
        arrived(mod_recv.at[src], mod1_s.at[k], mod1_r.at[src], sp=src)
    total = mod_recv[0]
    for s in range(1, n_sp):
        total = total + mod_recv[s]
    mod_part2 = mod_all.at[tp_i]
    mod_part2[...] = total
    for k in range(1, n_tp):
        send(
            mod_part2, mod_all.at[tp_i], mod2_s.at[k], mod2_r.at[tp_i], tp=(tp_i + k) % n_tp
        )
    for i in range(early, pieces):
        send_raw(i)
    for i in range(early):
        relay_raw(i)
    for k in range(1, n_tp):
        src = (tp_i + n_tp - k) % n_tp
        arrived(mod_all.at[src], mod2_s.at[k], mod2_r.at[src], tp=src)

    def modulate(x, which, start):
        at = pl.ds(start if isinstance(start, int) else pl.multiple_of(start, 16), x.shape[0])
        factor = lax.rsqrt(jnp.mean(x * x, axis=-1, keepdims=True) + norm_eps)
        for t in range(n_tp):
            cols = slice(t * mod_cols, (t + 1) * mod_cols)
            shift = mod_all[t, which : which + 1, :]
            scale = mod_all[t, which + 2 : which + 3, :]
            hidden[at, cols] = (
                (x[:, cols] * factor) * (1.0 + scale) + shift
            ).astype(bf16)

    half = 2 * own
    lane = lax.broadcasted_iota(jnp.int32, (half, LANES), 1)
    first_quarter = lane % HEAD_DIM < HEAD_DIM // 2
    low_half = lane < HEAD_DIM
    ctx_half = lax.broadcasted_iota(jnp.int32, (ctx_rows, LANES), 1) < HEAD_DIM

    def rope(u, rows):
        swapped = jnp.where(
            first_quarter,
            pltpu.roll(u, LANES - HEAD_DIM // 2, 1),
            pltpu.roll(u, HEAD_DIM // 2, 1),
        )
        return u * cos_t[rows, :] + swapped * sin_t[rows, :]

    def pair_up(a, b, low):
        return (
            jnp.where(low, a, pltpu.roll(b, HEAD_DIM, 1)).astype(bf16),
            jnp.where(low, pltpu.roll(a, HEAD_DIM, 1), b).astype(bf16),
        )

    def lat_slot(s, chip=None):
        if chip is None:
            return kv_buf.at[pl.ds(pl.multiple_of(s * tok, 16), tok)]
        return kv_buf.at[pl.ds(pl.multiple_of(s * tok + chip * half, 16), half)]

    def ctx_slot(s):
        return kv_buf.at[pl.ds(pl.multiple_of(n_sp * tok + s * ctx_rows, 16), ctx_rows)]

    order = list(range(1, groups))
    for c in range(chips):
        chip = (chip_i + c) % chips
        rows = pl.ds(pl.multiple_of(chip * half, 16), half)
        if c == 0:
            modulate(ctx[...].astype(f32), 1, half)
            modulate(raw[tp_i].astype(f32), 0, core_i * own)
            arrived(raw.at[partner], fwd_s.at[0, 0], fwd_r.at[chip_i, 0], tp=partner)
            modulate(raw[partner].astype(f32), 0, (1 - core_i) * own)
            for i in range(early, pieces):
                relay_raw(i)
            count = half + ctx_rows
        else:
            slot = chip * 2 + core_i
            modulate(raw[slot].astype(f32), 0, core_i * own)
            slot = chip * 2 + (1 - core_i)
            for i in range(pieces):
                arrived(
                    raw_piece(slot, i), fwd_s.at[chips - c, i], fwd_r.at[chip, i], tp=partner
                )
            modulate(raw[slot].astype(f32), 0, (1 - core_i) * own)
            count = half
        if c == 0:
            loads[0].wait()
        keys = [jnp.dot(hidden[:count, :], wk[m], preferred_element_type=f32) for m in (0, 1)]
        for p in range(groups // 2):
            slab = slice(p * LANES, (p + 1) * LANES)
            a, b = pair_up(
                rope(keys[0][:half, slab], rows), rope(keys[1][:half, slab], rows), low_half
            )
            kv_send[2 * p, rows, :LANES] = a
            kv_send[2 * p + 1, rows, :LANES] = b
            if c == 0:
                a, b = pair_up(keys[0][half:, slab], keys[1][half:, slab], ctx_half)
                kvc_send[2 * p, :, :LANES] = a
                kvc_send[2 * p + 1, :, :LANES] = b
        if c == 0:
            loads[1].wait()
        vals = jnp.dot(hidden[:count, :], wv[...], preferred_element_type=f32).astype(bf16)
        for j in range(groups):
            slab = slice(j * LANES, (j + 1) * LANES)
            kv_send[j, rows, LANES:] = vals[:half, slab]
            if c == 0:
                kvc_send[j, :, LANES:] = vals[half:, slab]
        for k in order:
            g = (g_i + k) % groups
            to = g * ranks + r_i
            send(
                kv_send.at[g, rows], lat_slot(sp_i, chip), kv_s.at[k, c], kv_r.at[g_i, c], sp=to
            )
            if c == 0:
                send(kvc_send.at[g], ctx_slot(sp_i), kvc_s.at[k], kvc_r.at[g_i], sp=to)
        for e in range(1, ranks):
            to = g_i * ranks + (r_i + e) % ranks
            send(
                kv_send.at[g_i, rows], lat_slot(sp_i, chip), rel_s.at[0, c, e],
                rel_r.at[g_i, c, r_i], sp=to,
            )
            if c == 0:
                send(
                    kvc_send.at[g_i], ctx_slot(sp_i), relc_s.at[0, e], relc_r.at[g_i, r_i], sp=to
                )
        if c == 0:
            loads[2].wait()
        queries = [
            jnp.dot(hidden[:half, :], wq[m], preferred_element_type=f32) for m in (0, 1)
        ]
        for p in range(groups // 2):
            slab = slice(p * LANES, (p + 1) * LANES)
            a, b = pair_up(
                rope(queries[0][:, slab], rows), rope(queries[1][:, slab], rows), low_half
            )
            q_send[2 * p, rows, :] = a
            q_send[2 * p + 1, rows, :] = b
    for k in order:
        g = (g_i + k) % groups
        send(q_send.at[g], q_buf.at[g_i], q_s.at[k], q_r.at[g_i], sp=g * ranks + r_i)
    local = [
        pltpu.make_async_copy(kv_send.at[g_i], lat_slot(sp_i), loc_sem.at[0]),
        pltpu.make_async_copy(kvc_send.at[g_i], ctx_slot(sp_i), loc_sem.at[1]),
        pltpu.make_async_copy(q_send.at[g_i], q_buf.at[g_i], loc_sem.at[2]),
    ]
    for copy in local:
        copy.start()

    for c in range(chips):
        chip = (chip_i + c) % chips
        for k in order:
            g = (g_i + groups - k) % groups
            s = g * ranks + r_i
            arrived(lat_slot(s, chip), kv_s.at[k, c], kv_r.at[g, c], sp=s)
            for e in range(1, ranks):
                to = g_i * ranks + (r_i + e) % ranks
                send(
                    lat_slot(s, chip), lat_slot(s, chip), rel_s.at[k, c, e],
                    rel_r.at[g, c, r_i], sp=to,
                )
            if c == 0:
                arrived(ctx_slot(s), kvc_s.at[k], kvc_r.at[g], sp=s)
                for e in range(1, ranks):
                    to = g_i * ranks + (r_i + e) % ranks
                    send(
                        ctx_slot(s), ctx_slot(s), relc_s.at[k, e], relc_r.at[g, r_i], sp=to
                    )
    for copy in local:
        copy.wait()
    for e in range(1, ranks):
        r = (r_i + ranks - e) % ranks
        to = g_i * ranks + r
        for k in range(groups):
            g = (g_i + groups - k) % groups
            s = g * ranks + r
            for c in range(chips):
                chip = (chip_i + c) % chips
                arrived(lat_slot(s, chip), rel_s.at[k, c, e], rel_r.at[g, c, r], sp=to)
            arrived(ctx_slot(s), relc_s.at[k, e], relc_r.at[g, r], sp=to)

    key_total = kv_buf.shape[0]
    q_tile = scores.shape[0] // 2
    block = pick(key_total, 512, LANES)
    coef = HEAD_DIM ** (-0.5) * 1.4426950408889634
    q_low = lax.broadcasted_iota(jnp.int32, (q_tile, LANES), 1) < HEAD_DIM
    head_lam = lam[g_i]
    tiles = tok // q_tile
    head_gain = gain[g_i]

    def attend(g, start):
        q = q_buf[g, pl.ds(start, q_tile), :]
        zero = jnp.zeros_like(q)
        q2 = jnp.concatenate([jnp.where(q_low, q, zero), jnp.where(q_low, zero, q)], axis=0)
        peak = None
        for b in range(key_total // block):
            rows = slice(b * block, (b + 1) * block)
            s = lax.dot_general(
                q2, kv_buf[rows, :LANES], (((1,), (1,)), ((), ())), preferred_element_type=f32
            )
            scores[:, rows] = s
            for c in range(block // LANES):
                piece = s[:, c * LANES : (c + 1) * LANES]
                peak = piece if peak is None else jnp.maximum(peak, piece)
        top = jnp.max(peak, axis=-1, keepdims=True) * coef
        sums = None
        acc = None
        for b in range(key_total // block):
            rows = slice(b * block, (b + 1) * block)
            w = jnp.exp2(scores[:, rows] * coef - top)
            for c in range(block // LANES):
                piece = w[:, c * LANES : (c + 1) * LANES]
                sums = piece if sums is None else sums + piece
            part = jnp.dot(w.astype(bf16), kv_buf[rows, LANES:], preferred_element_type=f32)
            acc = part if acc is None else acc + part
        mean_v = acc / jnp.sum(sums, axis=-1, keepdims=True)
        mixed = mean_v[:q_tile] - head_lam * mean_v[q_tile:]
        factor = lax.rsqrt(jnp.mean(mixed * mixed, axis=-1, keepdims=True) + norm_eps)
        o_send[g, pl.ds(start, q_tile), :] = (mixed * factor * head_gain).astype(bf16)

    def o_copy(k, i):
        g = (g_i + groups - k) % groups
        rows = pl.ds(pl.multiple_of(i * q_tile, 16), q_tile)
        return pltpu.make_async_remote_copy(
            src_ref=o_send.at[g, rows], dst_ref=heads.at[g_i, rows], send_sem=o_s.at[k, i],
            recv_sem=o_r.at[g_i, i], device_id={"sp": g * ranks + r_i}, device_id_type=MESH,
        )

    @pl.loop(0, groups)
    def _(k):
        g = (g_i + groups - k) % groups

        @pl.when(k > 0)
        def _():
            arrived(q_buf.at[g], q_s.at[k], q_r.at[g], sp=g * ranks + r_i)

        @pl.loop(0, tiles)
        def _(i):
            attend(g, pl.multiple_of(i * q_tile, q_tile))

            @pl.when(k > 0)
            def _():
                o_copy(k, i).start()

    heads[g_i] = o_send[g_i]
    loads[3].wait()
    for k in order:
        src = (g_i + k) % groups
        for i in range(tiles):
            rows = pl.ds(i * q_tile, q_tile)
            arrived(heads.at[src, rows], o_s.at[k, i], o_r.at[src, i], sp=src * ranks + r_i)

    parts = pair_send.shape[1]
    part_cols = width // parts

    def head_rows(chunk):
        start = pl.multiple_of(chunk * own, 16)
        return jnp.concatenate(
            [heads[h, pl.ds(start, own), :] for h in range(groups)], axis=-1
        )

    def term(left, p):
        cols = slice(p * part_cols, (p + 1) * part_cols)
        return jnp.dot(left, wo[:, cols], preferred_element_type=f32).astype(bf16)

    def to_partner(k):
        chip = (chip_i + 1 + k) % chips
        left = head_rows(chip * 2 + (1 - core_i))
        for p in range(parts):
            pair_send[k, p] = term(left, p)
            send(
                pair_send.at[k, p], pair_recv.at[k, p], pair_s.at[k, p], pair_r.at[k, p],
                tp=partner,
            )

    def with_partner(k):
        chip = (chip_i + 1 + k) % chips
        left = head_rows(chip * 2 + core_i)
        for p in range(parts):
            mine = term(left, p).astype(f32)
            arrived(pair_recv.at[k, p], pair_s.at[k, p], pair_r.at[k, p], tp=partner)
            both = mine + pair_recv[k, p].astype(f32)
            if k < chips - 1:
                fin_send[k, p] = both.astype(bf16)
                send(
                    fin_send.at[k, p], fin_recv.at[k, p], fin_s.at[k, p], fin_r.at[k, p],
                    tp=chip * 2 + core_i,
                )
            else:
                own_sum[p] = both

    for k in range(chips - 1):
        to_partner(k)
    for k in range(chips - 1):
        with_partner(k)
    to_partner(chips - 1)
    with_partner(chips - 1)
    for p in range(parts):
        summed = own_sum[p]
        for k in range(chips - 1):
            src_chip = (chip_i + chips - 1 - k) % chips
            arrived(
                fin_recv.at[k, p], fin_s.at[k, p], fin_r.at[k, p], tp=src_chip * 2 + core_i
            )
            summed = summed + fin_recv[k, p].astype(f32)
        cols = slice(p * part_cols, (p + 1) * part_cols)
        per = mod_cols // part_cols
        if per >= 1:
            low = (p % per) * part_cols
            gate = mod_all[p // per, 4:5, low : low + part_cols]
        else:
            span = part_cols // mod_cols
            gate = jnp.concatenate(
                [mod_all[p * span + q, 4:5, :] for q in range(span)], axis=-1
            )
        out[:, cols] = (lat[:, cols].astype(f32) + gate * summed).astype(bf16)
    for copy in pending:
        copy.wait_send()
    for k in order:
        for i in range(tiles):
            o_copy(k, i).wait_send()


def local(
    n_sp,
    n_tp,
    latent,
    context,
    cond_latent,
    cond_context,
    shift_weight,
    scale_weight,
    gate_weight,
    query_weight,
    key_weight,
    value_weight,
    out_weight,
    lambda_heads,
    out_gain,
):
    own, width = latent.shape
    ctx_rows = context.shape[0]
    tok = own * n_tp
    groups = lambda_heads.shape[0]
    ranks = n_sp // groups
    chips = n_tp // 2
    mod_rows, mod_cols = shift_weight.shape
    keys = n_sp * (tok + ctx_rows)
    q_tile = pick(tok, 128, 16)
    pieces = 3 if own % 48 == 0 else 1
    parts = 4 if width % (4 * LANES) == 0 else 1

    quarter = HEAD_DIM // 4
    inverse = np.float32(rope_theta) ** (-np.arange(quarter, dtype=np.float32) / quarter)
    zeros = np.zeros((quarter,), np.float32)
    repeat = LANES // (2 * quarter)
    half = np.ones((2 * quarter,), np.float32)
    lane_table = np.zeros((8, LANES), np.float32)
    lane_table[0] = np.tile(np.concatenate([inverse, zeros]), repeat)
    lane_table[1] = np.tile(np.concatenate([zeros, inverse]), repeat)
    lane_table[2] = np.tile(np.concatenate([-half, half]), repeat // 2)
    gain = out_gain.reshape(groups, 1, VALUE_DIM)
    vmem = pl.BlockSpec(memory_space=pltpu.VMEM)
    hbm = pl.BlockSpec(memory_space=pl.ANY)
    dma = pltpu.SemaphoreType.DMA
    scratch = [
        pltpu.VMEM(query_weight.shape, bf16),
        pltpu.VMEM(key_weight.shape, bf16),
        pltpu.VMEM(value_weight.shape, bf16),
        pltpu.VMEM(out_weight.shape, bf16),
        pltpu.VMEM((8, mod_cols), f32),
        pltpu.VMEM((n_sp, 8, mod_cols), f32),
        pltpu.VMEM((n_tp, 8, mod_cols), f32),
        pltpu.VMEM((n_tp, own, width), bf16),
        pltpu.VMEM((2 * own + ctx_rows, width), bf16),
        pltpu.VMEM((tok, LANES), f32),
        pltpu.VMEM((tok, LANES), f32),
        pltpu.VMEM((groups, tok, LANES), bf16),
        pltpu.VMEM((groups, tok, 2 * LANES), bf16),
        pltpu.VMEM((groups, ctx_rows, 2 * LANES), bf16),
        pltpu.VMEM((groups, tok, LANES), bf16),
        pltpu.VMEM((keys, 2 * LANES), bf16),
        pltpu.VMEM((2 * q_tile, keys), f32),
        pltpu.VMEM((groups, tok, LANES), bf16),
        pltpu.VMEM((groups, tok, LANES), bf16),
        pltpu.VMEM((chips, parts, own, width // parts), bf16),
        pltpu.VMEM((chips, parts, own, width // parts), bf16),
        pltpu.VMEM((max(chips - 1, 1), parts, own, width // parts), bf16),
        pltpu.VMEM((max(chips - 1, 1), parts, own, width // parts), bf16),
        pltpu.VMEM((parts, own, width // parts), f32),
        dma((4,)),
        dma((3,)),
        dma((n_sp,)),
        dma((n_sp,)),
        dma((n_tp,)),
        dma((n_tp,)),
        dma((chips, pieces)),
        dma((chips, pieces)),
        dma((chips, pieces)),
        dma((chips, pieces)),
        dma((groups,)),
        dma((groups,)),
        dma((groups, chips)),
        dma((groups, chips)),
        dma((groups,)),
        dma((groups,)),
        dma((groups, chips, ranks)),
        dma((groups, chips, ranks)),
        dma((groups, ranks)),
        dma((groups, ranks)),
        dma((groups, tok // q_tile)),
        dma((groups, tok // q_tile)),
        dma((chips, parts)),
        dma((chips, parts)),
        dma((chips, parts)),
        dma((chips, parts)),
    ]
    return pl.pallas_call(
        functools.partial(body, n_sp, n_tp),
        out_shape=jax.ShapeDtypeStruct((own, width), bf16),
        in_specs=[vmem] * 8 + [pl.BlockSpec(memory_space=pltpu.SMEM), vmem] + [hbm] * 4,
        out_specs=vmem,
        scratch_shapes=scratch,
        compiler_params=pltpu.CompilerParams(
            collective_id=0, has_side_effects=True, vmem_limit_bytes=60 * 1024 * 1024
        ),
        name="diff_attention",
    )(
        latent,
        context,
        cond_latent.reshape(n_sp, 1, mod_rows),
        cond_context.reshape(n_sp, 1, mod_rows),
        shift_weight,
        scale_weight,
        gate_weight,
        jnp.asarray(lane_table),
        lambda_heads,
        gain,
        query_weight,
        key_weight,
        value_weight,
        out_weight,
    )


def solution(mesh):
    placed = (
        P(("sp", "tp"), None),
        P("sp", None),
        P(),
        P(),
        P("sp", "tp"),
        P("sp", "tp"),
        P("sp", "tp"),
        P(None, None, "tp"),
        P(None, None, "tp"),
        P(None, "tp"),
        P("tp", None),
        P("tp"),
        P("tp"),
    )
    return jax.shard_map(
        functools.partial(local, mesh.shape["sp"], mesh.shape["tp"]),
        mesh=mesh,
        in_specs=placed,
        out_specs=P(("sp", "tp"), None),
        check_vma=False,
    )
```

time: 96.3 us -> 92.7 us (0.963)
  the two profiles are of different devices: /device:TPU:24 before, /device:TPU:0 now
where the time goes in v2:
time: 92.7 us; the launch traced here: 92.5 us
  Pallas kernels  90.7 us (98%)
  local copies, waits for them, and re-layouts  1.77 us (2%)
    pallas_call x1, Pallas kernels, local(): pl.pallas_call(functools.partial(body, n_sp, n_tp), out_shape=jax.ShapeDt...  90.7 us

profile of v2, /device:TPU:0, one launch (start us, length us, event | category | flops | bytes accessed | tf_op | source)
XLA Modules:
  0.0 92.5 jit_solution(17780735585983957353)
XLA Ops:
  0.0 90.7 %diff_attention.1 = bf16[96,2048]{1,0:T(8,128)(2,1)} custom-call(bf16[96,2048]{1,0:T(8,128)(2,1)} %lat.1, bf16[64,2048]{1,0:T(8,128)(2,1)} %ctx.1, f32[8,1,256]{2,1,0:T(1,128)} %bitcast.3, f32[8,1,256]{2,1,0:T(1,128)} %bitcast.4, bf16[256,512]{1,0:T(8,128)(2,1)} %shift_w.1, bf16[256,512]{1,0:T(8,128)(2,1)} %scale_w.1, bf16[256,512]{1,0:T(8,128)(2,1)} %gate_w.1, ...), custom_call_target="tpu_custom_call" | custom-call | tf_op jit(solution)/shard_map/diff_attention/pallas_call | solution.py:624
  90.7 1.8 %copy.16 = bf16[96,2048]{1,0:T(8,128)(2,1)} copy(bf16[96,2048]{1,0:T(8,128)(2,1)} %diff_attention.1) | data formatting | bytes 786432
